TPU v7x, 256 devices: a whole 4x4x8 slice. The times are simulated.
256 devices in a mesh: kv: 32 (over z, y), tp: 8 (over x, core).
Axes of the slice: x: 4, y: 4, z: 8, core: 2. Of those that a mesh axis runs over, the one named last changes fastest.
Arguments:
- tokens: bfloat16 [16, 4, 4096], P(None, None, 'kv'), may hold values from -20 to 20
- mix_gain: float32 [4096], P('kv'), may hold values from 0.1 to 1.9
- w_query: bfloat16 [4096, 2048], P('kv', 'tp'), may hold values from -0.09375 to 0.09375
- w_key: bfloat16 [4096, 2048], P('kv', 'tp'), may hold values from -0.09375 to 0.09375
- w_value: bfloat16 [4096, 2048], P('kv', 'tp'), may hold values from -0.09375 to 0.09375
- w_forget: bfloat16 [4096, 16], replicated, may hold values from -0.09375 to 0.09375
- forget_bias: float32 [16], P('tp'), may hold values from -1 to 3
- key_cache: bfloat16 [16, 16384, 2048], P(None, 'kv', 'tp'), may hold values from -6 to 6
- value_cache: bfloat16 [16, 16384, 2048], P(None, 'kv', 'tp'), may hold values from -6 to 6
- cum_gate: float32 [16, 16, 16384], P(None, 'tp', 'kv'), may hold values from -2236.08 to 0, as said below
- lengths: int32 [16], replicated, may hold values from 1 to 16384, 65524 in all
- w_out: bfloat16 [2048, 4096], P('tp', 'kv'), may hold values from -0.125 to 0.125
- mlp_gain: float32 [4096], P('kv'), may hold values from 0.1 to 1.9
- w_gate: bfloat16 [4096, 11264], P('kv', 'tp'), may hold values from -0.09375 to 0.09375
- w_up: bfloat16 [4096, 11264], P('kv', 'tp'), may hold values from -0.09375 to 0.09375
- w_down: bfloat16 [11264, 4096], P('tp', 'kv'), may hold values from -0.0546875 to 0.0546875
Outputs:
- result: bfloat16 [16, 4, 4096], P(None, None, 'kv')
Inputs may be any that keep to these rules, and one draw needn't show every extreme that they name: `cum_gate`: never rising along positions. `lengths`: one sequence fills all 16384 positions.
All inputs are finite; a program needn't handle non-finite values.
Results may differ from a plain program's by a relative error of at most 0.02.
Values may be sent and summed in bfloat16 or wider, within the bound.
A program may use at most 64 MiB of HBM per device.

v0:
```python
import jax
import jax.numpy as jnp
from jax import lax
from jax.sharding import Mesh
from jax.sharding import PartitionSpec as P

D = 4096
KV = ("kv_0", "kv_1")
EPSILON = 1e-06
NEG_FILL = -1e30


def in_one(arrays, axis):
    flat, at, outs = (jnp.concatenate([a.reshape(-1) for a in arrays]), 0, [])
    running = lax.psum(flat, axis)
    for a in arrays:
        outs.append(running[at : at + a.size].reshape(a.shape))
        at += a.size
    return tuple(outs)


def all_in_one(array, axis):
    leaves = jax.tree.leaves(array)
    turns = sorted(range(len(leaves)), key=lambda k: -leaves[k].size)
    width = (1, *leaves[turns[0]].shape)[-1]
    lines = [
        jnp.pad(leaves[k].reshape(-1), (0, -leaves[k].size % width)).reshape(-1, width)
        for k in turns
    ]
    both, at, found = (lax.all_gather(jnp.concatenate(lines), axis), 0, {})
    for k, line in zip(turns, lines):
        share = both[:, at : at + len(line)].reshape(len(both), -1)
        found[k] = share[:, : leaves[k].size].reshape(-1, *leaves[k].shape)
        at += len(line)
    numbers = iter(range(len(leaves)))
    return jax.tree.map(lambda _: found[next(numbers)], array)


def merged_by_axis(array, axes, combine):
    for axis in axes:
        pieces = all_in_one(array, axis)
        array = jax.tree.map(lambda part: part[0], pieces)
        for k in range(1, lax.axis_size(axis)):
            array = combine(array, jax.tree.map(lambda part: part[k], pieces))
    return array


def sent_to_all(array, axis):
    peers = lax.axis_size(axis)
    return lax.all_to_all(
        jnp.broadcast_to(array[None], (peers, *array.shape)), axis, 0, 0, tiled=True
    )


def of_everyone(array, axis):
    return sent_to_all(array, axis).astype(jnp.float32).sum(axis=0)


def over_copies(array, axis):
    everything = sent_to_all(array, axis)
    return jnp.sum(everything, axis=0)


def cut_along(array, dim, peers):
    shape = array.shape
    tiles = array.reshape(*shape[:dim], peers, shape[dim] // peers, *shape[dim + 1 :])
    return jnp.moveaxis(tiles, dim, 0)


def sum_at_owner(array, axis, dim):
    tiles = cut_along(array, dim, lax.axis_size(axis))
    arrived = lax.all_to_all(tiles, axis, split_axis=0, concat_axis=0, tiled=True)
    return arrived.astype(jnp.float32).sum(axis=0)


def sent_together(arrays, axis, dim, along):
    ends, at = ([], 0)
    for a in arrays[:-1]:
        at += a.shape[along]
        ends.append(at)
    both = jnp.concatenate(arrays, axis=along)
    return tuple(jnp.split(sum_at_owner(both, axis, dim), ends, axis=along))


def joined_along(tiles, dim):
    tiles = jnp.moveaxis(tiles, 0, dim)
    shape = tiles.shape
    return tiles.reshape(*shape[:dim], shape[dim] * shape[dim + 1], *shape[dim + 2 :])


def collect(array, axis, dim):
    tiles = sent_to_all(array, axis)
    return joined_along(tiles, dim)


def on_device(
    tokens,
    mix_gain,
    w_query,
    w_key,
    w_value,
    w_forget,
    forget_bias,
    key_cache,
    value_cache,
    cum_gate,
    lengths,
    w_out,
    mlp_gain,
    w_gate,
    w_up,
    w_down,
):
    seq_count, new_count, local_width = tokens.shape
    row_count = seq_count * new_count
    heads_dev = forget_bias.shape[0]
    head_width = w_query.shape[1] // heads_dev
    pos_dev = key_cache.shape[1]
    kv_index = lax.axis_index(KV)
    tp_index = lax.axis_index("tp")
    inputs = tokens.reshape(row_count, local_width).astype(jnp.float32)
    scaled = (inputs * mix_gain).astype(jnp.bfloat16)
    forget_rows = lax.dynamic_slice_in_dim(w_forget, kv_index * local_width, local_width, 0)
    forget_cols = lax.dynamic_slice_in_dim(forget_rows, tp_index * heads_dev, heads_dev, 1)
    query_part = jnp.dot(scaled, w_query, preferred_element_type=jnp.float32)
    key_part = jnp.dot(scaled, w_key, preferred_element_type=jnp.float32)
    value_part = jnp.dot(scaled, w_value, preferred_element_type=jnp.float32)
    forget_part = jnp.dot(scaled, forget_cols, preferred_element_type=jnp.float32)
    squares = jnp.sum(inputs * inputs, axis=1)
    query_sum, key_sum, value_sum, forget_sum, square_sum = tuple(
        (
            part.astype(jnp.float32)
            for part in in_one(
                (
                    query_part.astype(jnp.bfloat16),
                    key_part.astype(jnp.bfloat16),
                    value_part.astype(jnp.bfloat16),
                    forget_part.astype(jnp.bfloat16),
                    squares.astype(jnp.bfloat16),
                ),
                KV,
            )
        )
    )
    inv_norm = lax.rsqrt(square_sum / D + EPSILON)[:, None]
    head_shape = (seq_count, new_count, heads_dev, head_width)
    query = (inv_norm * query_sum).astype(jnp.bfloat16).reshape(head_shape)
    key_new = (inv_norm * key_sum).astype(jnp.bfloat16).reshape(head_shape)
    value_new = (inv_norm * value_sum).astype(jnp.bfloat16).reshape(head_shape)
    log_forget = jax.nn.log_sigmoid(inv_norm * forget_sum + forget_bias).reshape(
        seq_count, new_count, heads_dev
    )
    score_scale = head_width ** (-0.5)
    positions = kv_index * pos_dev + jnp.arange(pos_dev, dtype=jnp.int32)
    live_rows = positions[None, :] < lengths[:, None]
    live_mask = live_rows[:, None, None, :]
    cached_keys = key_cache.reshape(seq_count, pos_dev, heads_dev, head_width)
    cached_values = value_cache.reshape(seq_count, pos_dev, heads_dev, head_width)
    scores = jnp.einsum("bthd,bphd->bthp", query, cached_keys, preferred_element_type=jnp.float32)
    scores = scores * score_scale - cum_gate[:, None]
    scores = jnp.where(live_mask, scores, NEG_FILL)
    block_peak = jnp.max(scores, axis=3)
    weights = jnp.where(live_mask, jnp.exp(scores - block_peak[..., None]), 0.0)
    block_total = jnp.sum(weights, axis=3)
    block_sum = jnp.einsum(
        "bthp,bphd->bthd",
        weights.astype(jnp.bfloat16),
        cached_values,
        preferred_element_type=jnp.float32,
    )
    last_hit = positions[None, :] == (lengths - 1)[:, None]
    last_piece = jnp.sum(jnp.where(last_hit[:, None, :], cum_gate, 0.0), axis=2)

    def combine(first, second):
        peak_both = jnp.maximum(first[0], second[0])
        first_factor = jnp.exp(first[0] - peak_both)
        second_factor = jnp.exp(second[0] - peak_both)
        return (
            peak_both,
            first[1] * first_factor + second[1] * second_factor,
            first[2] * first_factor[..., None] + second[2] * second_factor[..., None],
            first[3] + second[3],
        )

    past_peak, past_total, past_sum, last_cum = merged_by_axis(
        (block_peak, block_total, block_sum, last_piece), KV, combine
    )
    key_cum = last_cum[:, None, :] + jnp.cumsum(log_forget, axis=1)
    own_scores = (
        jnp.einsum("bthd,bshd->bths", query, key_new, preferred_element_type=jnp.float32)
        * score_scale
    )
    own_scores = own_scores - jnp.transpose(key_cum, (0, 2, 1))[:, None]
    causal = (jnp.arange(new_count)[:, None] >= jnp.arange(new_count)[None, :])[None, :, None, :]
    own_scores = jnp.where(causal, own_scores, NEG_FILL)
    peak_score = jnp.maximum(past_peak, jnp.max(own_scores, axis=3))
    past_factor = jnp.exp(past_peak - peak_score)
    own_weights = jnp.where(causal, jnp.exp(own_scores - peak_score[..., None]), 0.0)
    numerator = past_sum * past_factor[..., None] + jnp.einsum(
        "bths,bshd->bthd",
        own_weights.astype(jnp.bfloat16),
        value_new,
        preferred_element_type=jnp.float32,
    )
    denominator = past_total * past_factor + jnp.sum(own_weights, axis=3)
    attended = (
        (numerator / denominator[..., None])
        .astype(jnp.bfloat16)
        .reshape(row_count, heads_dev * head_width)
    )
    attn_out = of_everyone(
        jnp.dot(attended, w_out, preferred_element_type=jnp.float32).astype(jnp.bfloat16), "tp"
    ).astype(jnp.float32)
    middle = (inputs + attn_out).astype(jnp.bfloat16)
    middle_wide = middle.astype(jnp.float32)
    squares2 = jnp.sum(middle_wide * middle_wide, axis=1)
    scaled2 = (middle_wide * mlp_gain).astype(jnp.bfloat16)
    gate_part = jnp.dot(scaled2, w_gate, preferred_element_type=jnp.float32)
    up_part = jnp.dot(scaled2, w_up, preferred_element_type=jnp.float32)
    kv_count = lax.axis_size(KV)
    share_rows = (row_count + kv_count - 1) // kv_count
    square_sum2 = over_copies(squares2, KV)
    gate_share, up_share = sent_together(
        (gate_part.astype(jnp.bfloat16), up_part.astype(jnp.bfloat16)), KV, 0, 1
    )
    share_squares = lax.dynamic_slice_in_dim(square_sum2, kv_index * share_rows, share_rows, 0)
    inv_norm2 = lax.rsqrt(share_squares / D + EPSILON)[:, None]
    hidden_share = (jax.nn.silu(inv_norm2 * gate_share) * (inv_norm2 * up_share)).astype(
        jnp.bfloat16
    )
    down_full = jnp.dot(collect(hidden_share, KV, 0), w_down, preferred_element_type=jnp.float32)
    mixed = of_everyone(down_full.astype(jnp.bfloat16), "tp").astype(jnp.float32)
    return (middle_wide + mixed).astype(jnp.bfloat16).reshape(seq_count, new_count, local_width)


def solution(mesh):
    split = Mesh(mesh.devices.reshape(8, 4, mesh.shape["tp"]), ("kv_0", "kv_1", "tp"))
    return jax.shard_map(
        on_device,
        mesh=split,
        in_specs=(
            P(None, None, KV),
            P(KV),
            P(KV, "tp"),
            P(KV, "tp"),
            P(KV, "tp"),
            P(),
            P("tp"),
            P(None, KV, "tp"),
            P(None, KV, "tp"),
            P(None, "tp", KV),
            P(),
            P("tp", KV),
            P(KV),
            P(KV, "tp"),
            P(KV, "tp"),
            P("tp", KV),
        ),
        out_specs=P(None, None, KV),
        check_vma=False,
    )
```

profile of v0, /device:TPU:1, one launch (start us, length us, event | category | flops | bytes accessed | tf_op | source)
XLA Modules:
  0.0 287.4 jit_solution(13230378988156012620)
XLA Ops:
  6.5 0.9 multiply_reduce_fusion
  7.5 0.7 multiply_convert_fusion.1
  8.3 0.9 convolution_convert_fusion.7
  9.4 1.0 fusion.23
  10.4 1.0 fusion.22
  11.5 1.0 fusion.21
  12.5 0.2 dynamic-update-slice.3
  12.7 0.2 dynamic-update-slice.4
  12.9 0.6 copy-done.4
  13.6 0.7 broadcast_add_fusion
  14.3 0.7 broadcast_compare_fusion.1
  15.0 1.0 select_reduce_fusion
  16.1 139.1 %all-reduce.4.cloned.1.call-done = bf16[49344]{0:T(1024)(128)(2,1)} async-done(((bf16[49344]{0:T(1024)(128)(2,1)}), bf16[49344]{0:T(1024)(128)(2,1)}) %all-reduce.4.cloned.1.call-update) | async-done | bytes 98704 | tf_op jit(solution)/shard_map/psum | solution.py:15
  155.2 0.7 fusion.103
  156.0 0.8 fusion.122
  157.0 3.5 %fusion.123 = (f32[16,4,2]{1,2,0:T(2,128)S(1)}, f32[16,4,2,512]{3,1,2,0:T(4,128)S(1)}) fusion(f32[16,2,512]{2,1,0:T(2,128)} %param.25, bf16[16,4,2,128]{3,0,2,1:T(8,128)(2,1)S(1)} %get-tuple-element.61, pred[16,512]{1,0:T(8,128)(4,1)S(1)} %get-tuple-element.62, bf16[16,512,256]{2,1,0:T(8,128)(2,1)} %param.23), kind=kOutput, calls=%fused_computation.233 | convolution fusion | flops 17039232 | bytes 4563456 | tf_op jit(solution)/shard_map/bthd,bphd->bthp/dot_general | solution.py:159
  160.5 0.2 copy.152
  160.7 0.3 fusion.24
  161.0 2.9 %fusion.18 = f32[16,4,2,128]{3,1,2,0:T(4,128)S(1)} fusion(f32[16,4,2,512]{3,1,2,0:T(4,128)S(1)} %get-tuple-element.65, f32[16,4,2]{1,2,0:T(2,128)S(1)} %get-tuple-element.64, pred[16,512]{1,0:T(8,128)(4,1)S(1)} %get-tuple-element.62, bf16[16,512,256]{2,1,0:T(8,128)(2,1)} %param.24), kind=kOutput, calls=%fused_computation.12 | convolution fusion | flops 16973824 | bytes 4530688 | tf_op jit(solution)/shard_map/bthp,bphd->bthd/dot_general | solution.py:165
  164.2 0.2 copy.153
  164.5 19.4 %all-gather.2 = f32[8,131,128]{2,1,0:T(8,128)S(1)} all-gather(f32[1,131,128]{2,1,0:T(8,128)S(1)} %maximum_bitcast_fusion), channel_id=2, replica_groups=mesh['kv_0'=8,'kv_1'=4,'tp'=8] {'kv_0'}, dimensions={0}, use_global_device_ids=true | all-gather | bytes 603648 | tf_op jit(solution)/shard_map/all_gather | solution.py:30
  184.1 0.3 fusion.31
  184.4 9.9 %all-gather.3 = f32[4,131,128]{2,1,0:T(8,128)S(1)} all-gather(f32[1,131,128]{2,1,0:T(8,128)S(1)} %maximum_bitcast_fusion.1), channel_id=3, replica_groups=mesh['kv_0'=8,'kv_1'=4,'tp'=8] {'kv_1'}, dimensions={0}, use_global_device_ids=true | all-gather | bytes 335360 | tf_op jit(solution)/shard_map/all_gather | solution.py:30
  194.4 0.7 slice_convert_fusion
  195.1 0.2 reshape.1214
  195.2 0.2 fusion.69
  196.0 0.2 squeeze.185
  196.2 0.2 squeeze.187
  196.5 0.2 squeeze.186
  196.8 0.2 squeeze.183
  197.1 0.2 squeeze.181
  197.4 0.2 squeeze.179
  197.6 0.2 squeeze.178
  198.8 0.2 fusion.52
  199.3 22.9 %all_to_all.26 = bf16[8,64,128]{2,1,0:T(8,128)(2,1)S(1)} all-to-all(bf16[8,64,128]{2,1,0:T(8,128)(2,1)S(1)} %broadcast_in_dim.71), channel_id=1, replica_groups=mesh['kv_0'=8,'kv_1'=4,'tp'=8] {'tp'}, dimensions={0} | all-to-all | bytes 262144 | tf_op jit(solution)/shard_map/all_to_all | solution.py:50
  222.4 0.6 broadcast_in_dim.73
  223.0 5.5 %all-to-all-start.1 = ((f32[32,1,64]{2,1,0:T(1,128)}), f32[32,1,64]{2,1,0:T(1,128)S(1)}, u32[]{:S(2)}, u32[]{:S(2)}) async-start(f32[32,1,64]{2,1,0:T(1,128)} %broadcast_in_dim.73), calls=%async_computation.1 | async-start | bytes 32768 | tf_op jit(solution)/shard_map/all_to_all | solution.py:50
  228.5 0.2 convolution_convert_fusion
  228.7 0.2 convolution_convert_fusion.1
  229.0 0.9 reshape.1208
  229.8 7.2 %all-to-all-done.1 = f32[32,1,64]{2,1,0:T(1,128)S(1)} async-done(((f32[32,1,64]{2,1,0:T(1,128)}), f32[32,1,64]{2,1,0:T(1,128)S(1)}, u32[]{:S(2)}, u32[]{:S(2)}) %all-to-all-start.1) | async-done | bytes 8224 | tf_op jit(solution)/shard_map/all_to_all | solution.py:50
  237.0 3.9 %all-to-all-start.2 = ((bf16[32,2,2816]{2,1,0:T(2,128)(2,1)}), bf16[32,2,2816]{2,1,0:T(2,128)(2,1)S(1)}, u32[]{:S(2)}, u32[]{:S(2)}) async-start(bf16[32,2,2816]{2,1,0:T(2,128)(2,1)} %reshape.1208), calls=%async_computation.2 | async-start | bytes 720896 | tf_op jit(solution)/shard_map/all_to_all | solution.py:72
  241.0 11.1 %all-to-all-done.2 = bf16[32,2,2816]{2,1,0:T(2,128)(2,1)S(1)} async-done(((bf16[32,2,2816]{2,1,0:T(2,128)(2,1)}), bf16[32,2,2816]{2,1,0:T(2,128)(2,1)S(1)}, u32[]{:S(2)}, u32[]{:S(2)}) %all-to-all-start.2) | async-done | bytes 360480 | tf_op jit(solution)/shard_map/all_to_all | solution.py:72
  252.1 0.3 convert_reduce_fusion
  252.6 15.6 %all_to_all.27 = bf16[32,2,1408]{2,1,0:T(2,128)(2,1)S(1)} all-to-all(bf16[32,2,1408]{2,1,0:T(2,128)(2,1)S(1)} %broadcast_in_dim.74), channel_id=1, replica_groups=mesh['kv_0'=8,'kv_1'=4,'tp'=8] {'kv_0','kv_1'}, dimensions={0} | all-to-all | bytes 360448 | tf_op jit(solution)/shard_map/all_to_all | solution.py:50
  268.3 0.2 convolution_convert_fusion.6
  268.5 11.4 %all_to_all.28 = bf16[8,64,128]{2,1,0:T(8,128)(2,1)S(1)} all-to-all(bf16[8,64,128]{2,1,0:T(8,128)(2,1)S(1)} %broadcast_in_dim.75), channel_id=1, replica_groups=mesh['kv_0'=8,'kv_1'=4,'tp'=8] {'tp'}, dimensions={0} | all-to-all | bytes 262144 | tf_op jit(solution)/shard_map/all_to_all | solution.py:50
  279.9 0.6 fusion.63
  (98 shorter events, 4.4 us)
Async XLA Ops:
  6.5 222.0 %copy-start = (bf16[128,1408]{1,0:T(8,128)(2,1)S(1)}, bf16[128,1408]{1,0:T(8,128)(2,1)}, u32[]{:S(2)}) copy-start(bf16[128,1408]{1,0:T(8,128)(2,1)} %param.30) | copy-start | bytes 1081348
  6.5 148.6 %all-reduce.4.cloned.1.call-start = ((), (), s32[]{:S(2)}) async-start(), calls=%async_computation.5 | async-start | bytes 200704 | tf_op jit(solution)/shard_map/psum | solution.py:15
  12.9 0.6 copy-start.4
  160.5 35.1 %copy-start.6 = (f32[2]{0:T(128)S(1)}, f32[2]{0:T(128)}, u32[]{:S(2)}) copy-start(f32[2]{0:T(128)} %param.22) | copy-start | bytes 28
  161.0 38.1 %copy-start.5 = (bf16[256,128]{1,0:T(8,128)(2,1)S(1)}, bf16[256,128]{1,0:T(8,128)(2,1)}, u32[]{:S(2)}) copy-start(bf16[256,128]{1,0:T(8,128)(2,1)} %param.27) | copy-start | bytes 196612
  161.0 61.2 %copy-start.3 = (bf16[16,4,128]{2,1,0:T(4,128)(2,1)S(1)}, bf16[16,4,128]{2,1,0:T(4,128)(2,1)}, u32[]{:S(2)}) copy-start(bf16[16,4,128]{2,1,0:T(4,128)(2,1)} %param.16) | copy-start | bytes 49156
  161.0 67.4 %copy-start.7 = (f32[128]{0:T(128)S(1)}, f32[128]{0:T(128)}, u32[]{:S(2)}) copy-start(f32[128]{0:T(128)} %param.28) | copy-start | bytes 1540
  164.0 64.7 %copy-start.1 = (bf16[128,1408]{1,0:T(8,128)(2,1)S(1)}, bf16[128,1408]{1,0:T(8,128)(2,1)}, u32[]{:S(2)}) copy-start(bf16[128,1408]{1,0:T(8,128)(2,1)} %param.29) | copy-start | bytes 1081348
  184.4 83.9 %copy-start.2 = (bf16[1408,128]{1,0:T(8,128)(2,1)S(1)}, bf16[1408,128]{1,0:T(8,128)(2,1)}, u32[]{:S(2)}) copy-start(bf16[1408,128]{1,0:T(8,128)(2,1)} %param.31) | copy-start | bytes 1081348
  223.0 14.0 %all-to-all-start.1 = ((f32[32,1,64]{2,1,0:T(1,128)}), f32[32,1,64]{2,1,0:T(1,128)S(1)}, u32[]{:S(2)}, u32[]{:S(2)}) async-start(f32[32,1,64]{2,1,0:T(1,128)} %broadcast_in_dim.73), calls=%async_computation.1 | async-start | bytes 32768 | tf_op jit(solution)/shard_map/all_to_all | solution.py:50
  237.0 15.1 %all-to-all-start.2 = ((bf16[32,2,2816]{2,1,0:T(2,128)(2,1)}), bf16[32,2,2816]{2,1,0:T(2,128)(2,1)S(1)}, u32[]{:S(2)}, u32[]{:S(2)}) async-start(bf16[32,2,2816]{2,1,0:T(2,128)(2,1)} %reshape.1208), calls=%async_computation.2 | async-start | bytes 720896 | tf_op jit(solution)/shard_map/all_to_all | solution.py:72
Sparse Core Ops, SparseCore 0:
  13.7 141.4 all-reduce.3
where the time goes:
time: 288 us; the launch traced here: 287 us
  waiting for transfers between devices  157 us (55%)
  blocking collectives  79.1 us (27%)
  between operations  14 us (5%)
  matrix products  11.2 us (4%)
  starting transfers between devices  9.34 us (3%)
  other arithmetic  8.2 us (3%)
  local copies, waits for them, and re-layouts  8.08 us (3%)
    psum x1, waiting for transfers between devices, in_one(): running = lax.psum(flat, axis)  139 us
    all_to_all x3, blocking collectives, sent_to_all(): lax.all_to_all(jnp.broadcast_to(array[None], (peers, *array.shape)), axis...  49.8 us
    all_gather x2, blocking collectives, all_in_one(): both, at, found = (lax.all_gather(jnp.concatenate(lines), axis), 0, {})  29.3 us
    all_to_all x1, waiting for transfers between devices, sum_at_owner(): lax.all_to_all(tiles, axis, split_axis=0, concat_axis=0, tiled=True)  11.1 us
    all_to_all x1, waiting for transfers between devices, sent_to_all(): lax.all_to_all(jnp.broadcast_to(array[None], (peers, *array.shape)), axis...  7.18 us
  transfers between devices with their start and end apart: 3, of which 3 were waited for; matrix products, arithmetic and copies ran while one was open for 1% of the time, Pallas kernels for 0%

commit v1 on v0

--- a/solution.py
+++ b/solution.py
@@ -12,7 +12,8 @@
 
 def in_one(arrays, axis):
     flat, at, outs = (jnp.concatenate([a.reshape(-1) for a in arrays]), 0, [])
-    running = lax.psum(flat, axis)
+    blocks = lax.all_gather(flat, axis, axis=0, tiled=False)
+    running = blocks.sum(axis=0)
     for a in arrays:
         outs.append(running[at : at + a.size].reshape(a.shape))
         at += a.size

time: 288 us -> 318 us (1.10)
  waiting for transfers between devices: 157 us -> 177 us
  local copies, waits for them, and re-layouts: 8.08 us -> 17.5 us
    unnamed x1 -> x2, waiting for transfers between devices: 0.02 us -> 158 us
    psum x1 -> x0, waiting for transfers between devices: 139 us -> none  [in_one(): running = lax.psum(flat, axis)]
    unnamed x23 -> x32, local copies, waits for them, and re-layouts: 1.05 us -> 6.39 us
    all_gather x0 -> x1, local copies, waits for them, and re-layouts: none -> 4.05 us  [in_one(): blocks = lax.all_gather(flat, axis, axis=0, tiled=False)]
where the time goes in v1:
time: 318 us; the launch traced here: 317 us
  waiting for transfers between devices  177 us (56%)
  blocking collectives  78.9 us (25%)
  local copies, waits for them, and re-layouts  17.5 us (6%)
  between operations  14.7 us (5%)
  matrix products  11.2 us (4%)
  starting transfers between devices  9.22 us (3%)
  other arithmetic  8.83 us (3%)
    unnamed x2, waiting for transfers between devices  158 us
    all_to_all x3, blocking collectives, sent_to_all(): lax.all_to_all(jnp.broadcast_to(array[None], (peers, *array.shape)), axis...  49.5 us
    all_gather x2, blocking collectives, all_in_one(): both, at, found = (lax.all_gather(jnp.concatenate(lines), axis), 0, {})  29.5 us
    all_to_all x1, waiting for transfers between devices, sum_at_owner(): lax.all_to_all(tiles, axis, split_axis=0, concat_axis=0, tiled=True)  11.1 us
    all_to_all x1, waiting for transfers between devices, sent_to_all(): lax.all_to_all(jnp.broadcast_to(array[None], (peers, *array.shape)), axis...  7.64 us
    unnamed x32, local copies, waits for them, and re-layouts  6.39 us
  transfers between devices with their start and end apart: 3, of which 3 were waited for; matrix products, arithmetic and copies ran while one was open for 1% of the time, Pallas kernels for 0%

profile of v1, /device:TPU:1, one launch (start us, length us, event | category | flops | bytes accessed | tf_op | source)
XLA Modules:
  0.0 317.0 jit_solution(4360595918905964072)
XLA Ops:
  6.5 0.9 multiply_reduce_fusion
  7.4 1.3 multiply_convert_fusion.1
  8.8 1.0 fusion.21
  9.8 1.0 fusion.22
  10.8 1.0 fusion.23
  11.8 0.9 convolution_convert_fusion.7
  13.1 1.3 dynamic-slice
  15.1 0.2 dynamic-update-slice.4
  15.3 0.2 dynamic-update-slice.5
  15.5 0.6 copy-done.5
  16.1 0.2 broadcast.123
  16.4 2.2 dynamic-update-slice
  18.5 1.7 copy-done.1
  20.4 1.0 select_reduce_fusion
  21.4 157.9 %all-reduce.5.cloned.1.call-done = bf16[1579008]{0:T(1024)(128)(2,1)} async-done(((bf16[1579008]{0:T(1024)(128)(2,1)}), bf16[1579008]{0:T(1024)(128)(2,1)}) %all-reduce.5.cloned.1.call-update) | async-done | bytes 3158032
  179.3 4.1 %reshape.1218 = bf16[32,49344]{1,0:T(8,128)(2,1)S(1)} reshape(bf16[1579008]{0:T(1024)(128)(2,1)} %all-reduce.5.cloned.1.call-done) | data formatting | bytes 6316032 | tf_op jit(solution)/shard_map/all_gather | solution.py:15
  183.4 1.4 reduce_sum.98
  184.7 0.7 slice_convert_fusion
  185.4 0.7 fusion.103
  186.1 0.8 fusion.122
  187.2 3.5 %fusion.123 = (f32[16,4,2]{1,2,0:T(2,128)S(1)}, f32[16,4,2,512]{3,1,2,0:T(4,128)S(1)}) fusion(f32[16,2,512]{2,1,0:T(2,128)} %param.25, bf16[16,4,2,128]{3,0,2,1:T(8,128)(2,1)S(1)} %get-tuple-element.61, pred[16,512]{1,0:T(8,128)(4,1)S(1)} %get-tuple-element.62, bf16[16,512,256]{2,1,0:T(8,128)(2,1)} %param.23), kind=kOutput, calls=%fused_computation.233 | convolution fusion | flops 17039232 | bytes 4563456 | tf_op jit(solution)/shard_map/bthd,bphd->bthp/dot_general | solution.py:160
  190.7 0.2 copy.152
  190.9 0.3 fusion.24
  191.2 0.2 copy.153
  191.7 2.9 fusion.18
  194.7 19.9 %all-gather.3 = f32[8,131,128]{2,1,0:T(8,128)S(1)} all-gather(f32[1,131,128]{2,1,0:T(8,128)S(1)} %maximum_bitcast_fusion), channel_id=3, replica_groups=mesh['kv_0'=8,'kv_1'=4,'tp'=8] {'kv_0'}, dimensions={0}, use_global_device_ids=true | all-gather | bytes 603648 | tf_op jit(solution)/shard_map/all_gather | solution.py:31
  214.8 0.3 fusion.31
  215.2 9.5 %all-gather.4 = f32[4,131,128]{2,1,0:T(8,128)S(1)} all-gather(f32[1,131,128]{2,1,0:T(8,128)S(1)} %maximum_bitcast_fusion.1), channel_id=4, replica_groups=mesh['kv_0'=8,'kv_1'=4,'tp'=8] {'kv_1'}, dimensions={0}, use_global_device_ids=true | all-gather | bytes 335360 | tf_op jit(solution)/shard_map/all_gather | solution.py:31
  225.9 0.2 squeeze.181
  226.5 0.2 squeeze.179
  227.4 0.2 squeeze.187
  227.7 0.2 squeeze.186
  227.9 0.2 squeeze.185
  228.5 0.2 fusion.52
  228.9 22.5 %all_to_all.26 = bf16[8,64,128]{2,1,0:T(8,128)(2,1)S(1)} all-to-all(bf16[8,64,128]{2,1,0:T(8,128)(2,1)S(1)} %broadcast_in_dim.71), channel_id=1, replica_groups=mesh['kv_0'=8,'kv_1'=4,'tp'=8] {'tp'}, dimensions={0} | all-to-all | bytes 262144 | tf_op jit(solution)/shard_map/all_to_all | solution.py:51
  251.5 0.2 convolution_convert_fusion
  251.7 0.2 convolution_convert_fusion.1
  252.1 0.6 broadcast_in_dim.73
  252.8 5.3 %all-to-all-start.1 = ((f32[32,1,64]{2,1,0:T(1,128)}), f32[32,1,64]{2,1,0:T(1,128)S(1)}, u32[]{:S(2)}, u32[]{:S(2)}) async-start(f32[32,1,64]{2,1,0:T(1,128)} %broadcast_in_dim.73), calls=%async_computation.1 | async-start | bytes 32768 | tf_op jit(solution)/shard_map/all_to_all | solution.py:51
  258.1 0.9 reshape.1208
  259.0 7.6 %all-to-all-done.1 = f32[32,1,64]{2,1,0:T(1,128)S(1)} async-done(((f32[32,1,64]{2,1,0:T(1,128)}), f32[32,1,64]{2,1,0:T(1,128)S(1)}, u32[]{:S(2)}, u32[]{:S(2)}) %all-to-all-start.1) | async-done | bytes 8224 | tf_op jit(solution)/shard_map/all_to_all | solution.py:51
  266.6 3.9 %all-to-all-start.2 = ((bf16[32,2,2816]{2,1,0:T(2,128)(2,1)}), bf16[32,2,2816]{2,1,0:T(2,128)(2,1)S(1)}, u32[]{:S(2)}, u32[]{:S(2)}) async-start(bf16[32,2,2816]{2,1,0:T(2,128)(2,1)} %reshape.1208), calls=%async_computation.2 | async-start | bytes 720896 | tf_op jit(solution)/shard_map/all_to_all | solution.py:73
  270.6 11.1 %all-to-all-done.2 = bf16[32,2,2816]{2,1,0:T(2,128)(2,1)S(1)} async-done(((bf16[32,2,2816]{2,1,0:T(2,128)(2,1)}), bf16[32,2,2816]{2,1,0:T(2,128)(2,1)S(1)}, u32[]{:S(2)}, u32[]{:S(2)}) %all-to-all-start.2) | async-done | bytes 360480 | tf_op jit(solution)/shard_map/all_to_all | solution.py:73
  281.8 0.3 convert_reduce_fusion
  282.3 15.6 %all_to_all.27 = bf16[32,2,1408]{2,1,0:T(2,128)(2,1)S(1)} all-to-all(bf16[32,2,1408]{2,1,0:T(2,128)(2,1)S(1)} %broadcast_in_dim.74), channel_id=1, replica_groups=mesh['kv_0'=8,'kv_1'=4,'tp'=8] {'kv_0','kv_1'}, dimensions={0} | all-to-all | bytes 360448 | tf_op jit(solution)/shard_map/all_to_all | solution.py:51
  297.9 0.2 convolution_convert_fusion.6
  298.1 11.4 %all_to_all.28 = bf16[8,64,128]{2,1,0:T(8,128)(2,1)S(1)} all-to-all(bf16[8,64,128]{2,1,0:T(8,128)(2,1)S(1)} %broadcast_in_dim.75), channel_id=1, replica_groups=mesh['kv_0'=8,'kv_1'=4,'tp'=8] {'tp'}, dimensions={0} | all-to-all | bytes 262144 | tf_op jit(solution)/shard_map/all_to_all | solution.py:51
  309.6 0.6 fusion.63
  (109 shorter events, 5.1 us)
Async XLA Ops:
  6.5 245.0 %copy-start = (bf16[128,1408]{1,0:T(8,128)(2,1)S(1)}, bf16[128,1408]{1,0:T(8,128)(2,1)}, u32[]{:S(2)}) copy-start(bf16[128,1408]{1,0:T(8,128)(2,1)} %param.30) | copy-start | bytes 1081348
  6.5 13.7 %copy-start.10 = (s32[16]{0:T(128)S(1)}, s32[16]{0:T(128)}, u32[]{:S(2)}) copy-start(s32[16]{0:T(128)} %param.26) | copy-start | bytes 196
  6.5 172.8 %all-reduce.5.cloned.1.call-start = ((), (), s32[]{:S(2)}) async-start(), calls=%async_computation.5 | async-start | bytes 6316032
  15.5 0.6 copy-start.5
  18.5 1.7 copy-start.1
  190.7 34.3 %copy-start.8 = (f32[2]{0:T(128)S(1)}, f32[2]{0:T(128)}, u32[]{:S(2)}) copy-start(f32[2]{0:T(128)} %param.22) | copy-start | bytes 28
  191.7 37.1 %copy-start.7 = (bf16[256,128]{1,0:T(8,128)(2,1)S(1)}, bf16[256,128]{1,0:T(8,128)(2,1)}, u32[]{:S(2)}) copy-start(bf16[256,128]{1,0:T(8,128)(2,1)} %param.27) | copy-start | bytes 196612
  191.7 59.8 %copy-start.6 = (f32[64,128]{1,0:T(8,128)S(1)}, f32[64,128]{1,0:T(8,128)}, u32[]{:S(2)}) copy-start(f32[64,128]{1,0:T(8,128)} %get-tuple-element.34) | copy-start | bytes 98308
  191.7 59.8 %copy-start.9 = (f32[128]{0:T(128)S(1)}, f32[128]{0:T(128)}, u32[]{:S(2)}) copy-start(f32[128]{0:T(128)} %param.28) | copy-start | bytes 1540
  194.7 57.1 %copy-start.2 = (bf16[128,1408]{1,0:T(8,128)(2,1)S(1)}, bf16[128,1408]{1,0:T(8,128)(2,1)}, u32[]{:S(2)}) copy-start(bf16[128,1408]{1,0:T(8,128)(2,1)} %param.29) | copy-start | bytes 1081348
  194.7 57.3 %copy-start.4 = (bf16[16,4,128]{2,1,0:T(4,128)(2,1)S(1)}, bf16[16,4,128]{2,1,0:T(4,128)(2,1)}, u32[]{:S(2)}) copy-start(bf16[16,4,128]{2,1,0:T(4,128)(2,1)} %param.16) | copy-start | bytes 49156
  215.1 82.8 %copy-start.3 = (bf16[1408,128]{1,0:T(8,128)(2,1)S(1)}, bf16[1408,128]{1,0:T(8,128)(2,1)}, u32[]{:S(2)}) copy-start(bf16[1408,128]{1,0:T(8,128)(2,1)} %param.31) | copy-start | bytes 1081348
  252.8 13.9 %all-to-all-start.1 = ((f32[32,1,64]{2,1,0:T(1,128)}), f32[32,1,64]{2,1,0:T(1,128)S(1)}, u32[]{:S(2)}, u32[]{:S(2)}) async-start(f32[32,1,64]{2,1,0:T(1,128)} %broadcast_in_dim.73), calls=%async_computation.1 | async-start | bytes 32768 | tf_op jit(solution)/shard_map/all_to_all | solution.py:51
  266.6 15.1 %all-to-all-start.2 = ((bf16[32,2,2816]{2,1,0:T(2,128)(2,1)}), bf16[32,2,2816]{2,1,0:T(2,128)(2,1)S(1)}, u32[]{:S(2)}, u32[]{:S(2)}) async-start(bf16[32,2,2816]{2,1,0:T(2,128)(2,1)} %reshape.1208), calls=%async_computation.2 | async-start | bytes 720896 | tf_op jit(solution)/shard_map/all_to_all | solution.py:73
Sparse Core Ops, SparseCore 0:
  20.4 158.8 all-reduce.4
